TPU v7x, 128 devices: a whole 4x4x4 slice. The times are simulated.
128 devices in a mesh: ep: 64 (over z, y, x), tp: 2 (over core).
Axes of the slice: x: 4, y: 4, z: 4, core: 2. Of those that a mesh axis runs over, the one named last changes fastest.
Arguments:
- tokens: bfloat16 [16384, 2048], P('ep'), may hold values from -16 to 16
- expert_ids: int32 [16384, 4], P('ep'), may hold values from 0 to 63, all different within a row; in each aligned block of 256 rows (0 to 255, 256 to 511, ...) at most 24 rows name the same one
- gates: float32 [16384, 4], P('ep'), may hold values from 0.05 to 0.6
- cotangent: bfloat16 [16384, 2048], P('ep'), may hold values from -16 to 16
- w_gate: bfloat16 [64, 2048, 512], P('ep', None, 'tp'), may hold values from -0.125 to 0.125
- w_up: bfloat16 [64, 2048, 512], P('ep', None, 'tp'), may hold values from -0.125 to 0.125
- w_down: bfloat16 [64, 512, 2048], P('ep', 'tp'), may hold values from -0.25 to 0.25
- sh_gate: bfloat16 [2048, 512], P(None, 'tp'), may hold values from -0.125 to 0.125
- sh_up: bfloat16 [2048, 512], P(None, 'tp'), may hold values from -0.125 to 0.125
- sh_down: bfloat16 [512, 2048], P('tp'), may hold values from -0.25 to 0.25
Outputs:
- token_grad: bfloat16 [16384, 2048], P('ep', 'tp')
- gate_grad: float32 [16384, 4], P('ep')
- expert_gate_grad: float32 [64, 2048, 512], P('ep', None, 'tp')
- expert_up_grad: float32 [64, 2048, 512], P('ep', None, 'tp')
- expert_down_grad: float32 [64, 512, 2048], P('ep', 'tp')
- shared_gate_grad: float32 [2048, 512], P('ep', 'tp')
- shared_up_grad: float32 [2048, 512], P('ep', 'tp')
- shared_down_grad: float32 [512, 2048], P('tp', 'ep')
- expert_gate_rows: float32 [64, 2048], P('ep')
- expert_up_rows: float32 [64, 2048], P('ep')
- expert_down_rows: float32 [64, 512], P('ep', 'tp')
- shared_gate_rows: float32 [2048], P('ep')
- shared_up_rows: float32 [2048], P('ep')
- shared_down_rows: float32 [512], P('tp')
Inputs may be any that keep to these rules, and one draw needn't show every extreme that they name: `expert_ids`: each row names 4 different experts. Within each aligned block of 256 tokens no expert is named by more than 24 assignments, a bound that is reached in some blocks.
All inputs are finite; a program needn't handle non-finite values.
Results may differ from a plain program's by a relative error of at most 0.0085.
Values may be sent and summed in bfloat16 or wider, within the bound.
A program may use at most 128 MiB of HBM per device.

v0:
```python
import functools

import jax
import jax.numpy as jnp
from jax import lax
from jax.experimental import pallas as pl
from jax.experimental.pallas import tpu as pltpu
from jax.sharding import PartitionSpec as P

F32 = jnp.float32
BF16 = jnp.bfloat16
MESH_ID = pl.DeviceIdType.MESH
CAP = 24
NEP = 64
CHUNKS = 4
BLK = NEP // CHUNKS
ROWS = NEP * CAP
CR = BLK * CAP


AXES = ((2, 1, 0), (1, 0, 2), (0, 2, 1))
WIDE = (768, 512, 768)
BACK = (384, 384, 256)
B_AT = (0, 384, 768)
R_AT = (0, 768, 1280)
ORDER = (0, 1, 3, 2)


def place(me):
    return lax.rem(me, 4), lax.rem(lax.div(me, 4), 4), lax.div(me, 16)


def shifted(me, offs):
    x, y, z = (lax.rem(c + o, 4) for c, o in zip(place(me), offs))
    return z * 16 + y * 4 + x


def target(me, k):
    return shifted(me, place(k))


def origin(me, k):
    return shifted(me, tuple(4 - o for o in place(k)))


def nn(a, b):
    return lax.dot_general(a, b, (((1,), (0,)), ((), ())), preferred_element_type=F32)


def nt(a, b):
    return lax.dot_general(a, b, (((1,), (1,)), ((), ())), preferred_element_type=F32)


def tn(a, b):
    return lax.dot_general(a, b, (((0,), (0,)), ((), ())), preferred_element_type=F32)


def nonlinear(gp, up, hc):
    s = jax.nn.sigmoid(gp)
    act = gp * s
    slope = s * (1.0 + gp * (1.0 - s))
    hid = (act * up).astype(BF16)
    dg = (hc * up * slope).astype(BF16)
    du = (hc * act).astype(BF16)
    return hid, dg, du


def kernel(
    ids, gates, order, tok_h, cot_h, wg_h, wu_h, wd_h, sg_h, su_h, sd_h,
    o_tok, o_gate, o_rank, o_gg, o_gu, o_gd, o_nrm, o_dn, o_rs, o_sn, o_sdn,
    meta, meta_in, pick, slot_gate, tok, cot, wg, wu, wd, sg, su, sd,
    raw, b0, b1, b2, c0, c1, c2, w0, w1, w2, v0, v1, v2,
    hid_b, dg_b, du_b, rc0, rc1, rc2, rb0, rb1, rb2, s_r0, s_r1, s_r2,
    gpart, gother, g1, g2, g3, stage, nrm, nrm_o, sn, sn_o,
    sh_own, sh_give, sh_got, sh_sum, r0, r1, r2, q0, q1, q2, p1, p2, p3, dnb,
    a_s, a_r, i_s, i_r, d_s, d_r, k_s, k_r, f_s, f_r, x_s, x_r,
    b_s, b_r, y_s, y_r, z_s, z_r, l_s,
    g_s, g_r, t_s, t_r, n_s, n_r, st_s, e_s, e_r, w_s,
):
    out_b, mid, own, oth = (b0, b1, b2), (c0, c1, c2), (w0, w1, w2), (v0, v1, v2)
    rc, rb, s_r = (rc0, rc1, rc2), (rb0, rb1, rb2), (s_r0, s_r1, s_r2)
    me = lax.axis_index("ep")
    h = lax.axis_index("tp")
    mx, my, mz = place(me)
    mate = {"tp": 1 - h}
    width = tok.shape[1] // 2
    half = width // 2

    loads = [
        pltpu.make_async_copy(a, b, w_s.at[i])
        for i, (a, b) in enumerate(
            ((tok_h, tok), (cot_h, cot), (sg_h, sg), (su_h, su), (sd_h, sd), (wg_h, wg), (wu_h, wu), (wd_h, wd))
        )
    ]
    for cp in loads:
        cp.start()
    bar = pltpu.get_barrier_semaphore()

    def axis_peer(axis, d):
        x, y, z = mx, my, mz
        if axis == 0:
            x = lax.rem(x + d, 4)
        elif axis == 1:
            y = lax.rem(y + d, 4)
        else:
            z = lax.rem(z + d, 4)
        return x, y, z, z * 16 + y * 4 + x

    def peer(axis, d):
        return {"ep": axis_peer(axis, d)[3]}

    for axis in range(3):
        for d in range(1, 4):
            pl.semaphore_signal(bar, inc=1, device_id=peer(axis, d), device_id_type=MESH_ID)
    pl.semaphore_signal(bar, inc=1, device_id=mate, device_id_type=MESH_ID)

    def remote(src, dst, s, r, dev):
        return pltpu.make_async_remote_copy(
            src_ref=src, dst_ref=dst, send_sem=s, recv_sem=r, device_id=dev, device_id_type=MESH_ID
        )

    def flat(v):
        return v.reshape(-1, v.shape[-1])

    def blocks(v, *lead):
        return v.reshape(*lead, CAP, v.shape[-1])

    every = slice(None)

    def col(lo, n):
        return pl.ds(pl.multiple_of(h * width + lo, 128), n)

    raw_parts = (
        (0, tok, 0, 768, 0), (1, tok, 768, 256, 0), (1, cot, 0, 256, 256), (2, cot, 256, 768, 0),
    )

    def gather_copies(d):
        cps = []
        for i, (q, src, lo, n, at) in enumerate(raw_parts):
            cps.append((q, remote(
                src.at[:, col(lo, n)], raw.at[pl.ds((d - 1) * 256, 256), pl.ds(R_AT[q] + at, n)],
                a_s.at[d - 1, i], a_r.at[d - 1, i], peer(AXES[q][0], d),
            )))
        return cps

    def meta_copy(q, d):
        return remote(
            meta.at[q, d], meta_in.at[q, d - 1], i_s.at[q, d - 1], i_r.at[q, d - 1], peer(AXES[q][0], d)
        )

    def first_copy(q, d, e):
        return remote(
            out_b[q].at[e - 1, d], mid[q].at[d, e],
            d_s.at[q, d, e - 1], d_r.at[q, d, e - 1], peer(AXES[q][1], e),
        )

    def second_copies(q, c):
        out = []
        for g in (1, 3, 2, 0) if q != 1 else (c,):
            m, o = mid[q], own[q]
            src = (m.at[c, :, g], m.at[:, :, c], m.at[:, c, g])[q]
            dst = (o.at[c, :, g], o.at[c], o.at[c, g])[q]
            if g == 0:
                out.append((g, pltpu.make_async_copy(src, dst, k_s.at[q, c, 0])))
            else:
                out.append((g, remote(src, dst, k_s.at[q, c, g], k_r.at[q, c, g], peer(AXES[q][2], g))))
        return out

    def forward(q, c):
        return remote(own[q].at[c], oth[q].at[c], f_s.at[q, c], f_r.at[q, c], mate)

    firsts = set()

    def second(q, c):
        for d in (c,) if q == 0 else range(4):
            for e in (c,) if q == 2 else range(4):
                if e > 0 and (q, d, e) not in firsts:
                    firsts.add((q, d, e))
                    first_copy(q, d, e).wait_recv()
        for _, cp in second_copies(q, c):
            cp.start()

    n_tok = tok.shape[0]
    earlier = lax.broadcasted_iota(jnp.int32, (n_tok, n_tok), 0)
    later = lax.broadcasted_iota(jnp.int32, (n_tok, n_tok), 1)
    before = jnp.where(later > earlier, 1.0, 0.0).astype(BF16)
    for q in range(3):
        named = jnp.zeros((NEP, n_tok), F32)
        gate_t = jnp.zeros((NEP, n_tok), F32)
        for j in range(4):
            hit = ids[j:j + 1] == order[q]
            named = jnp.where(hit, 1.0, named)
            gate_t = jnp.where(hit, gates[j:j + 1], gate_t)
        rank_t = jnp.where(named > 0.0, nn(named.astype(BF16), before), -1.0)
        if q == 0:
            o_rank[...] = rank_t
        for d in range(4):
            meta[q, d, 0] = rank_t[d * 16:(d + 1) * 16]
            meta[q, d, 1] = gate_t[d * 16:(d + 1) * 16]

    for cp in loads[:2]:
        cp.wait()
    pl.semaphore_wait(bar, 10)
    sends = []
    for d in (1, 3, 2):
        for q in range(3):
            sends.append(meta_copy(q, d))
        sends.extend(cp for _, cp in gather_copies(d))
    n_near = 2 * len(sends) // 3
    for cp in sends[:n_near]:
        cp.start()

    slot_no = lax.broadcasted_iota(jnp.int32, (CAP, n_tok), 0).astype(F32)

    def place_rows(q, d, with_gate):
        ref = meta.at[q, 0] if d == 0 else meta_in.at[q, d - 1]
        for k in range(16):
            filled = ref[0, k:k + 1] == slot_no
            pick[k * CAP:(k + 1) * CAP] = jnp.where(filled, 1.0, 0.0).astype(BF16)
            if with_gate:
                slot_gate[k * CAP:(k + 1) * CAP] = jnp.sum(
                    jnp.where(filled, ref[1, k:k + 1], 0.0), axis=1, keepdims=True
                )

    def put(q, d, cols, v):
        v = blocks(v, 4, 4).astype(BF16)
        mid[q][d, 0, :, :, cols] = v[0]
        for e in range(1, 4):
            out_b[q][e - 1, d, :, :, cols] = v[e]

    for cp in loads[2:]:
        cp.wait()
    gp = nn(tok[...], sg[...])
    up = nn(tok[...], su[...])
    hc = nt(cot[...], sd[...])
    s_hid, s_dg, s_du = nonlinear(gp, up, hc)
    tile = 512
    tiles = tok.shape[1] // tile
    for i in range(tiles):
        cs = slice(i * tile, (i + 1) * tile)
        t_t = tok[:, cs]
        r0[i] = tn(t_t, s_dg).astype(BF16)
        r1[i] = tn(t_t, s_du).astype(BF16)
        r2[4 * i:4 * i + 4] = tn(cot[:, cs], s_hid).astype(BF16).reshape(4, 128, 256)

    def rs_copies(phase):
        out = []
        for d in (1, 3, 2):
            for a in range(3):
                axis = AXES[a][phase]
                x, y, z, dev = axis_peer(axis, d)
                if phase == 0:
                    src = (r0.at[z], r1.at[:, pl.ds(pl.multiple_of(y * 128, 128), 128)],
                           r2.at[:, pl.ds(pl.multiple_of(x * 32, 32), 32)])[a]
                    dst = (q0, q1, q2)[a].at[d - 1]
                elif phase == 1:
                    src = (p1.at[0, pl.ds(pl.multiple_of(y * 4, 4), 4)], p1.at[1, pl.ds(pl.multiple_of(x * 4, 4), 4)],
                           p1.at[2, pl.ds(pl.multiple_of(z * 4, 4), 4)])[a]
                    dst = p2.at[a, d]
                else:
                    src = p2.at[a, 0, (x, z, y)[a]]
                    dst = p3.at[a, d - 1]
                i = (phase * 3 + d - 1) * 3 + a
                out.append(remote(src, dst, t_s.at[i], t_r.at[i], {"ep": dev}))
        return out

    def produce(d):
        for q in range(3):
            if d > 0:
                meta_copy(q, d).wait_recv()
                for qq, cp in gather_copies(d):
                    if qq == q:
                        cp.wait_recv()
            place_rows(q, d, q > 0)
            for qq, src, lo, n, at in raw_parts:
                if qq != q:
                    continue
                for j in range(0, n, 256):
                    if d == 0:
                        x = src[:, col(lo + j, 256)]
                    else:
                        x = raw[(d - 1) * 256:d * 256, R_AT[q] + at + j:R_AT[q] + at + j + 256]
                    v = nn(pick[...], x)
                    if src is cot:
                        v = slot_gate[...] * v
                    put(q, d, slice(at + j, at + j + 256), v)
            for e in range(1, 4):
                first_copy(q, d, e).start()

    produce(0)
    for cp in sends[n_near:]:
        cp.start()
    for i in range(2):
        cols = pl.ds(pl.multiple_of(h * width + i * half, 128), half)
        r = pl.ds(pl.multiple_of(h * width + i * half, 128), half)
        sh_own[:, i * half:(i + 1) * half] = (
            nt(s_dg, sg[r]) + nt(s_du, su[r])
        ).astype(BF16)
        r = pl.ds(pl.multiple_of((1 - h) * width + i * half, 128), half)
        sh_give[:, i * half:(i + 1) * half] = (
            nt(s_dg, sg[r]) + nt(s_du, su[r])
        ).astype(BF16)
    sh_cp = remote(sh_give, sh_got, e_s.at[0], e_r.at[0], mate)
    sh_cp.start()

    produce(1)
    produce(3)
    produce(2)
    rs0 = rs_copies(0)
    second(2, 0)
    second(0, 0)

    for q, c in ((1, 0), (0, 1), (1, 1), (1, 3), (2, 1), (1, 2), (0, 3), (2, 3)):
        second(q, c)

    def arrive(c):
        for q in range(3):
            for g, cp in second_copies(q, c):
                if g > 0:
                    cp.wait_recv()
                else:
                    cp.wait()
            forward(q, c).start()

    def cross(c):
        out = []
        for i in range(4):
            buf, at = give_at(c, i)
            dst = raw.at[pl.ds((c // 2) * CR, CR), pl.ds((c % 2) * width + i * 256, 256)]
            out.append(remote(buf.at[pl.ds(at, CR)], dst, x_s.at[c, i], x_r.at[c, i], mate))
        return out

    def give_at(c, i):
        n = ORDER.index(c) % 2 * 4 + i
        return (sg, su)[n // 5], n % 5 * CR

    def back_at(q, c):
        if q == 0:
            return out_b[0], c % 3, 384 * (c // 3)
        if c == 3:
            return out_b[2], q - 1 if q == 1 else 1, 256
        return out_b[q], c, 0

    def rows_of(base, lo, n):
        return pl.ds(pl.multiple_of(base * width + lo, 128), n)

    def compute(c):
        rows = pl.ds(c * CR, CR)
        for q in range(3):
            forward(q, c).wait_recv()
        gp = up = hc = None
        for base, buf in ((h, own), (1 - h, oth)):
            for lo, n, x in ((0, 768, flat(buf[0][c])), (768, 256, flat(buf[1][c, :, :, :, :256]))):
                r = rows_of(base, lo, n)
                g, u = nn(x, wg[r]), nn(x, wu[r])
                gp, up = (g, u) if gp is None else (gp + g, up + u)
            for lo, n, x in ((0, 256, flat(buf[1][c, :, :, :, 256:])), (256, 768, flat(buf[2][c]))):
                t = nt(x, wd[:, rows_of(base, lo, n)])
                hc = t if hc is None else hc + t
        hid, dg, du = nonlinear(gp, up, hc)
        hid_b[rows] = hid
        dg_b[rows] = dg
        du_b[rows] = du
        gsum = jnp.sum(hid.astype(F32) * hc, axis=1, keepdims=True).reshape(BLK, CAP, 1)
        lane = lax.broadcasted_iota(jnp.int32, (BLK, CAP, 128), 2)
        rank = lax.broadcasted_iota(jnp.int32, (BLK, CAP, 128), 1)
        packed = jnp.sum(jnp.where(lane == rank, gsum, 0.0), axis=1)
        for i in range(BLK):
            gpart[c, i // 4, i % 4] = packed[i:i + 1]
        if ORDER.index(c) >= 2:
            for cp in cross(ORDER[ORDER.index(c) - 2]):
                cp.wait_send()
        for i, cp in enumerate(cross(c)):
            buf, at = give_at(c, i)
            r = pl.ds(pl.multiple_of((1 - h) * width + i * 256, 256), 256)
            buf[at:at + CR] = (nt(dg, wg[r]) + nt(du, wu[r])).astype(BF16)
            cp.start()
        for q in range(3):
            r = rows_of(h, B_AT[q], BACK[q])
            buf, b, lo = back_at(q, c)
            buf[b, :, :, :, lo:lo + BACK[q]] = blocks(nt(dg, wg[r]) + nt(du, wu[r]), 4, 4).astype(BF16)

    def back_copies(q, c):
        out = []
        buf, b, lo = back_at(q, c)
        src = buf.at[b, :, :, :, pl.ds(lo, BACK[q])]
        for g in (1, 3, 2, 0) if q != 1 else (c,):
            s_g = (src.at[:, g], src, src.at[g])[q]
            v = rc[q]
            dst = (v.at[c, :, g], v.at[:, :, c], v.at[:, c, g])[q]
            if g == 0:
                out.append((g, pltpu.make_async_copy(s_g, dst, l_s.at[q, c])))
            else:
                to = peer(AXES[q][2], 4 - g)
                out.append((g, remote(s_g, dst, b_s.at[q, c, g], b_r.at[q, c, g], to)))
        return out

    def finish(c):
        for cp in cross(c):
            cp.wait_recv()
        for q in range(3):
            n = BACK[q]
            buf, b, lo = back_at(q, c)
            at = c % 2 * width + B_AT[q]
            buf[b, :, :, :, lo:lo + n] = (
                buf[b, :, :, :, lo:lo + n].astype(F32)
                + blocks(raw[(c // 2) * CR:(c // 2 + 1) * CR, at:at + n].astype(F32), 4, 4)
            ).astype(BF16)
        for q in range(3):
            for _, cp in back_copies(q, c):
                cp.start()

    def back2_copies(q, c):
        out = []
        v, w = rc[q], rb[q]
        for e in (1, 3, 2, 0) if q != 2 else (c,):
            at = ((c, e), (every, e, c), (every, e))[q]
            if e == 0:
                out.append((e, pltpu.make_async_copy(v.at[at], w.at[at], l_s.at[q, 4 + c])))
            else:
                to = peer(AXES[q][1], 4 - e)
                out.append((e, remote(v.at[at], w.at[at], y_s.at[q, c, e], y_r.at[q, c, e], to)))
        return out

    def legs(c):
        for q in (1, 2, 0):
            for g, cp in back_copies(q, c):
                if g > 0:
                    cp.wait_recv()
                else:
                    cp.wait()
            for _, cp in back2_copies(q, c):
                cp.start()

    for q in range(3):
        for d in range(4):
            for e in range(1, 4):
                first_copy(q, d, e).wait_send()
    for n, c in enumerate(ORDER):
        arrive(c)
        for q, cc in ((), ((0, 2), (2, 2)), (), ())[n]:
            second(q, cc)
        for a in ((), (0,), (1, 2), ())[n]:
            for cp in rs0[a::3]:
                cp.start()
        if n >= 1:
            finish(ORDER[n - 1])
        compute(c)
        if n == 2:
            legs(0)
    g_cp = remote(gpart, gother, e_s.at[1], e_r.at[1], mate)
    g_cp.start()
    finish(ORDER[-1])
    legs(1)

    def leg2_done(q, c):
        for e, cp in back2_copies(q, c):
            if e > 0:
                cp.wait_recv()
            else:
                cp.wait()

    def back3_copy(q, d):
        return remote(
            raw.at[pl.ds((d - 1) * 256, 256), pl.ds(R_AT[q], BACK[q])], s_r[q].at[d - 1],
            z_s.at[q, d], z_r.at[q, d], peer(AXES[q][0], 4 - d),
        )

    def leg3(q, d):
        place_rows(q, d, False)
        v = tn(pick[...], flat(rb[q][d]))
        if d > 0:
            raw[(d - 1) * 256:d * 256, R_AT[q]:R_AT[q] + BACK[q]] = v.astype(BF16)
            back3_copy(q, d).start()
        else:
            sh_sum[:, B_AT[q]:B_AT[q] + BACK[q]] = v

    def near_rows():
        for d in (0, 1, 3):
            leg2_done(0, d)
            leg3(0, d)

    def far_rows():
        for q in (1, 2):
            for c in ORDER:
                leg2_done(q, c)
            for d in (1, 3, 2, 0):
                leg3(q, d)
        leg2_done(0, 2)
        leg3(0, 2)

    def f(v):
        return v.astype(F32)

    def scatter2():
        for cp in rs0:
            cp.wait()
        s0 = f(r0[mz]) + f(q0[0]) + f(q0[1]) + f(q0[2])
        p1[0] = s0.reshape(16, 32, 256).astype(BF16)
        s1 = (f(r1[:, pl.ds(pl.multiple_of(my * 128, 128), 128)]) + f(q1[0]) + f(q1[1]) + f(q1[2])).reshape(4, 4, 32, 256)
        for i in range(4):
            for j in range(4):
                p1[1, 4 * j + i] = s1[i, j].astype(BF16)
        s2 = f(r2[:, pl.ds(pl.multiple_of(mx * 32, 32), 32)]) + f(q2[0]) + f(q2[1]) + f(q2[2])
        p1[2] = s2.astype(BF16)
        for cp in rs_copies(1):
            cp.start()

    def scatter3():
        for cp in rs_copies(1):
            cp.wait()
        for a in range(3):
            own_i = (my, mx, mz)[a]
            p2[a, 0] = (
                f(p1[a, pl.ds(pl.multiple_of(own_i * 4, 4), 4)]) + f(p2[a, 1]) + f(p2[a, 2]) + f(p2[a, 3])
            ).astype(BF16)
        for cp in rs_copies(2):
            cp.start()

    gates_on = (gother, g1, g2, g3)

    def gate_copies(leg):
        out = []
        for g in range(1, 4):
            at = ((every, every, g), (every, g), (g,))[leg]
            src, dst = gates_on[leg].at[at], gates_on[leg + 1].at[at]
            out.append(remote(src, dst, g_s.at[leg, g], g_r.at[leg, g], peer(leg, 4 - g)))
        return out

    def gate_leg(leg):
        if leg == 0:
            g_cp.wait()
            gother[...] = gpart[...] + gother[...]
        else:
            for cp in gate_copies(leg - 1):
                cp.wait()
        at = ((every, every, 0), (every, 0), (0,))[leg]
        gates_on[leg + 1][at] = gates_on[leg][at]
        for cp in gate_copies(leg):
            cp.start()

    sn_cp = remote(sn, sn_o, e_s.at[3], e_r.at[3], mate)

    def spread(leg):
        return [
            remote(dnb.at[leg, 0], dnb.at[leg, g], n_s.at[leg, g], n_r.at[leg, g], peer(leg, g))
            for g in range(1, 4)
        ]

    def spread_leg(leg):
        if leg > 0:
            for cp in spread(leg - 1):
                cp.wait()
            dnb[leg, 0] = dnb[leg - 1, 0] + dnb[leg - 1, 1] + dnb[leg - 1, 2] + dnb[leg - 1, 3]
        if leg < 3:
            for cp in spread(leg):
                cp.start()

    def scatter_end():
        for cp in rs_copies(2):
            cp.wait()
        for a in range(3):
            own_i = (mx, mz, my)[a]
            v = f(p2[a, 0, own_i]) + f(p3[a, 0]) + f(p3[a, 1]) + f(p3[a, 2])
            o_rs[a] = v
            if a < 2:
                sn[a] = jnp.broadcast_to(jnp.sum(v * v, axis=1, keepdims=True), (32, 128))
            else:
                dnb[0, 0] = jnp.sum(v * v, axis=0, keepdims=True)
        sn_cp.start()
        spread_leg(0)

    ones = jnp.ones((8, 256), F32)

    def row_norm(g):
        return lax.dot_general(
            ones, g * g, (((1,), (1,)), ((), ())), preferred_element_type=F32, precision=lax.Precision.HIGHEST
        )

    n_t = width // 256

    def stage_copies(step, slot, f0):
        fr = pl.ds(f0, 256)
        return (
            pltpu.make_async_copy(stage.at[slot, 0], o_gg.at[fr], st_s.at[slot, 0]),
            pltpu.make_async_copy(stage.at[slot, 1], o_gu.at[fr], st_s.at[slot, 1]),
            pltpu.make_async_copy(stage.at[slot, 2], o_gd.at[:, fr], st_s.at[slot, 2]),
        )

    hid_all = hid_b[...]
    dn = jnp.zeros((8, 256), F32)
    pending = [None, None]
    AFTER = {
        0: (functools.partial(legs, 3), functools.partial(gate_leg, 0)),
        1: (functools.partial(legs, 2), scatter2),
        2: (near_rows, functools.partial(gate_leg, 1)),
        3: (far_rows, scatter3),
        4: (functools.partial(gate_leg, 2),),
        5: (scatter_end,),
        6: (functools.partial(spread_leg, 1),),
        7: (functools.partial(spread_leg, 2),),
    }
    for step in range(2 * n_t):
        slot = step % 2
        buf = own if step < n_t else oth
        i = step % n_t
        base = h if step < n_t else 1 - h
        f0 = pl.multiple_of(base * width + i * 256, 256)
        if pending[slot] is not None:
            for cp in pending[slot]:
                cp.wait()
        lhs = flat(buf[0][..., i * 256:(i + 1) * 256] if i < 3 else buf[1][..., :256])
        rhs = flat(buf[1][..., 256:] if i == 0 else buf[2][..., (i - 1) * 256:i * 256])
        grad1 = tn(lhs, dg_b[...])
        stage[slot, 0] = grad1
        nrm[0:8, pl.ds(f0, 256)] = row_norm(grad1)
        grad2 = tn(lhs, du_b[...])
        stage[slot, 1] = grad2
        nrm[8:16, pl.ds(f0, 256)] = row_norm(grad2)
        grad3 = tn(hid_all, rhs)
        stage[slot, 2] = grad3
        dn = dn + row_norm(grad3)
        pending[slot] = stage_copies(step, slot, f0)
        for cp in pending[slot]:
            cp.start()
        for fn in AFTER.get(step, ()):
            fn()
    o_dn[...] = dn
    nrm_cp = remote(nrm, nrm_o, e_s.at[2], e_r.at[2], mate)
    nrm_cp.start()

    nrm_cp.wait()
    o_nrm[...] = nrm[...] + nrm_o[...]
    sn_cp.wait()
    o_sn[...] = sn[...] + sn_o[...]
    sh_cp.wait()
    for cp in gate_copies(2):
        cp.wait()
    for k in range(NEP):
        o_gate[k:k + 1] = g3[k // 16, k // 4 % 4, k % 4]
    for q in range(3):
        cs = slice(B_AT[q], B_AT[q] + BACK[q])
        v = sh_sum[:, cs] + (f(sh_own[:, cs]) + f(sh_got[:, cs]))
        for d in range(1, 4):
            back3_copy(q, d).wait()
            v = v + f(s_r[q][d - 1])
        o_tok[:, cs] = v.astype(BF16)

    spread_leg(3)
    o_sdn[...] = dnb[3, 0]
    for cp in sends:
        cp.wait_send()
    for q in range(3):
        for c in range(CHUNKS):
            forward(q, c).wait_send()
            for g, cp in second_copies(q, c) + back_copies(q, c):
                if g > 0:
                    cp.wait_send()
            for e, cp in back2_copies(q, c):
                if e > 0:
                    cp.wait_send()
    for c in ORDER[2:]:
        for cp in cross(c):
            cp.wait_send()
    for cps in pending:
        for cp in cps:
            cp.wait()


def tail(
    ids, gates, order, rank, gate_sum, tok_in, nrm, dn, rs, sn, sdn, gg, gu, gd,
    o_tok, o_gate, o_gg, o_gu, o_gd, o_sg, o_su, o_sd, o_gn, o_un, o_dn, o_sgn, o_sun, o_sdn,
    bg, bu, bd, i_s, o_s,
):
    rows = bd.shape[0]
    parts = []
    for a, (src, buf, dst) in enumerate(((gg, bg, o_gg), (gu, bu, o_gu))):
        for i in range(2):
            r = pl.ds(i * 1024, 1024)
            parts.append((src.at[r], buf.at[r], dst.at[0, r]))
    for i in range(2):
        r = pl.ds(i * 128, 128)
        parts.append((gd.at[r], bd.at[r], o_gd.at[0, r]))
    ins = [pltpu.make_async_copy(a, b, i_s.at[i]) for i, (a, b, _) in enumerate(parts)]
    outs = [pltpu.make_async_copy(b, c, o_s.at[i]) for i, (_, b, c) in enumerate(parts)]
    for cp in ins:
        cp.start()
    o_tok[...] = tok_in[...]
    value = jnp.zeros(rank.shape, F32)
    for r in range(CAP):
        value = jnp.where(rank[...] == float(r), gate_sum[:, r:r + 1], value)
    for j in range(4):
        hit = ids[j:j + 1] == order[0]
        total = jnp.sum(jnp.where(hit, value, 0.0), axis=0, keepdims=True)
        o_gate[j:j + 1] = total / gates[j:j + 1]
    o_sg[...] = rs[0]
    o_su[...] = rs[1]
    o_sd[...] = rs[2].T
    o_gn[...] = nrm[0:1]
    o_un[...] = nrm[8:9]
    o_dn[...] = dn[0:1]
    o_sgn[...] = sn[0].T[0:1]
    o_sun[...] = sn[1].T[0:1]
    o_sdn[...] = sdn[...]
    for a, b in zip(ins, outs):
        a.wait()
        b.start()
    for b in outs:
        b.wait()


def local(tokens, expert_ids, gates, cotangent, w_gate, w_up, w_down, sh_gate, sh_up, sh_down):
    me = lax.axis_index("ep")
    rows, width = tokens.shape
    k = lax.broadcasted_iota(jnp.int32, (NEP, 1), 0)
    dist = place(k)[::-1]
    order = jnp.stack(
        [shifted(me, tuple(dist[AXES[q].index(axis)] for axis in range(3))) for q in range(3)]
    )
    ids_t, gates_t = expert_ids.T, gates.T

    vm = pl.BlockSpec(memory_space=pltpu.VMEM)
    hbm = pl.BlockSpec(memory_space=pl.ANY)
    half = width // 2
    dma = pltpu.SemaphoreType.DMA
    out = pl.pallas_call(
        kernel,
        out_shape=(
            jax.ShapeDtypeStruct((rows, half), BF16),
            jax.ShapeDtypeStruct((NEP, 128), F32),
            jax.ShapeDtypeStruct((NEP, rows), F32),
            jax.ShapeDtypeStruct((width, 256), F32),
            jax.ShapeDtypeStruct((width, 256), F32),
            jax.ShapeDtypeStruct((256, width), F32),
            jax.ShapeDtypeStruct((16, width), F32),
            jax.ShapeDtypeStruct((8, 256), F32),
            jax.ShapeDtypeStruct((3, 32, 256), F32),
            jax.ShapeDtypeStruct((2, 32, 128), F32),
            jax.ShapeDtypeStruct((1, 256), F32),
        ),
        in_specs=[vm] * 3 + [hbm] * 8,
        out_specs=(vm, vm, vm, hbm, hbm, hbm, vm, vm, vm, vm, vm),
        scratch_shapes=[
            pltpu.VMEM((3, 4, 2, 16, rows), F32),
            pltpu.VMEM((3, 3, 2, 16, rows), F32),
            pltpu.VMEM((CR, rows), BF16),
            pltpu.VMEM((CR, 1), F32),
            pltpu.VMEM((rows, width), BF16),
            pltpu.VMEM((rows, width), BF16),
            pltpu.VMEM((width, 256), BF16),
            pltpu.VMEM((width, 256), BF16),
            pltpu.VMEM((256, width), BF16),
            pltpu.VMEM((width, 256), BF16),
            pltpu.VMEM((width, 256), BF16),
            pltpu.VMEM((256, width), BF16),
            pltpu.VMEM((3 * rows, width), BF16),
            *[pltpu.VMEM((3, 4, 4, CAP, n), BF16) for n in WIDE],
            *[pltpu.VMEM((4, 4, 4, CAP, n), BF16) for n in WIDE],
            *[pltpu.VMEM((4, 4, 4, CAP, n), BF16) for n in WIDE],
            *[pltpu.VMEM((4, 4, 4, CAP, n), BF16) for n in WIDE],
            pltpu.VMEM((ROWS, 256), BF16),
            pltpu.VMEM((ROWS, 256), BF16),
            pltpu.VMEM((ROWS, 256), BF16),
            *[pltpu.VMEM((4, 4, 4, CAP, n), BF16) for n in BACK],
            *[pltpu.VMEM((4, 4, 4, CAP, n), BF16) for n in BACK],
            *[pltpu.VMEM((3, rows, n), BF16) for n in BACK],
            *[pltpu.VMEM((4, 4, 4, 1, 128), F32)] * 5,
            pltpu.VMEM((2, 3, 256, 256), F32),
            pltpu.VMEM((16, width), F32),
            pltpu.VMEM((16, width), F32),
            pltpu.VMEM((2, 32, 128), F32),
            pltpu.VMEM((2, 32, 128), F32),
            pltpu.VMEM((rows, half), BF16),
            pltpu.VMEM((rows, half), BF16),
            pltpu.VMEM((rows, half), BF16),
            pltpu.VMEM((rows, half), F32),
            pltpu.VMEM((4, 512, 256), BF16),
            pltpu.VMEM((4, 512, 256), BF16),
            pltpu.VMEM((16, 128, 256), BF16),
            pltpu.VMEM((3, 512, 256), BF16),
            pltpu.VMEM((3, 4, 128, 256), BF16),
            pltpu.VMEM((3, 16, 32, 256), BF16),
            pltpu.VMEM((3, 16, 32, 256), BF16),
            pltpu.VMEM((3, 4, 4, 32, 256), BF16),
            pltpu.VMEM((3, 3, 32, 256), BF16),
            pltpu.VMEM((4, 4, 1, 256), F32),
            dma((3, 4)), dma((3, 4)),
            dma((3, 3)), dma((3, 3)),
            dma((3, 4, 3)), dma((3, 4, 3)),
            dma((3, 4, 4)), dma((3, 4, 4)),
            dma((3, 4)), dma((3, 4)),
            dma((CHUNKS, 4)), dma((CHUNKS, 4)),
            dma((3, CHUNKS, 4)), dma((3, CHUNKS, 4)),
            dma((3, CHUNKS, 4)), dma((3, CHUNKS, 4)),
            dma((3, 4)), dma((3, 4)),
            dma((3, 8)),
            dma((3, 4)), dma((3, 4)),
            dma((27,)), dma((27,)),
            dma((3, 4)), dma((3, 4)),
            dma((2, 3)),
            dma((4,)), dma((4,)),
            dma((8,)),
        ],
        compiler_params=pltpu.CompilerParams(
            collective_id=0, has_side_effects=True, vmem_limit_bytes=67043328
        ),
    )(ids_t, gates_t, order, tokens, cotangent, w_gate[0], w_up[0], w_down[0], sh_gate, sh_up, sh_down)
    tok_grad, gate_sum, rank, gg, gu, gd, nrm, dn, rs, sn, sdn = out
    res = pl.pallas_call(
        tail,
        out_shape=(
            jax.ShapeDtypeStruct((rows, half), BF16),
            jax.ShapeDtypeStruct((4, rows), F32),
            jax.ShapeDtypeStruct((1, width, 256), F32),
            jax.ShapeDtypeStruct((1, width, 256), F32),
            jax.ShapeDtypeStruct((1, 256, width), F32),
            jax.ShapeDtypeStruct((32, 256), F32),
            jax.ShapeDtypeStruct((32, 256), F32),
            jax.ShapeDtypeStruct((256, 32), F32),
            jax.ShapeDtypeStruct((1, width), F32),
            jax.ShapeDtypeStruct((1, width), F32),
            jax.ShapeDtypeStruct((1, 256), F32),
            jax.ShapeDtypeStruct((1, 32), F32),
            jax.ShapeDtypeStruct((1, 32), F32),
            jax.ShapeDtypeStruct((1, 256), F32),
        ),
        in_specs=[vm] * 11 + [hbm] * 3,
        out_specs=(vm, vm, hbm, hbm, hbm) + (vm,) * 9,
        scratch_shapes=[
            pltpu.VMEM((width, 256), F32),
            pltpu.VMEM((width, 256), F32),
            pltpu.VMEM((256, width), F32),
            dma((6,)), dma((6,)),
        ],
    )(ids_t, gates_t, order, rank, gate_sum, tok_grad, nrm, dn, rs, sn, sdn, gg, gu, gd)
    return (res[0], res[1].T) + res[2:11] + (res[11][0], res[12][0], res[13][0])


def solution(mesh):
    placed = (
        P("ep", None),
        P("ep", None),
        P("ep", None),
        P("ep", None),
        P("ep", None, "tp"),
        P("ep", None, "tp"),
        P("ep", "tp", None),
        P(None, "tp"),
        P(None, "tp"),
        P("tp", None),
    )
    return jax.shard_map(
        local,
        mesh=mesh,
        in_specs=placed,
        out_specs=(
            P("ep", "tp"),
            P("ep", None),
            P("ep", None, "tp"),
            P("ep", None, "tp"),
            P("ep", "tp", None),
            P("ep", "tp"),
            P("ep", "tp"),
            P("tp", "ep"),
            P("ep", None),
            P("ep", None),
            P("ep", "tp"),
            P("ep"),
            P("ep"),
            P("tp"),
        ),
        check_vma=False,
    )
```

profile of v0, /device:TPU:0, one launch (start us, length us, event | category | flops | bytes accessed | tf_op | source)
XLA Modules:
  0.0 147.3 jit_solution(4850273510294332715)
XLA Ops:
  0.7 0.8 copy.26.order
  1.5 136.6 %shard_map.209 = (bf16[256,1024]{1,0:T(8,128)(2,1)}, f32[64,128]{1,0:T(8,128)}, f32[64,256]{1,0:T(8,128)}, f32[2048,256]{1,0:T(8,128)}, f32[2048,256]{1,0:T(8,12...) custom-call(s32[4,256]{1,0:T(4,128)} %bitcast.12, ...), custom_call_target="tpu_custom_call" | custom-call | tf_op jit(solution)/shard_map/pallas_call | solution.py:726
  138.1 7.6 %shard_map.210 = (bf16[256,1024]{1,0:T(8,128)(2,1)}, f32[4,256]{1,0:T(4,128)}, f32[1,2048,256]{2,1,0:T(8,128)}, f32[1,2048,256]{2,1,0:T(8,128)}, f32[1,256,2048]...) custom-call(s32[4,256]{1,0:T(4,128)} %bitcast.13, ...), custom_call_target="tpu_custom_call" | custom-call | tf_op jit(solution)/shard_map/pallas_call | solution.py:809
  145.7 1.6 %copy.27 = f32[256,32]{0,1:T(8,128)} copy(f32[256,32]{1,0:T(8,128)} %get-tuple-element.85) | data formatting | bytes 65536
  (3 shorter events, 0.0 us)
where the time goes:
time: 148 us; the launch traced here: 147 us
  Pallas kernels  144 us (97%)
  local copies, waits for them, and re-layouts  2.36 us (2%)
    pallas_call x1, Pallas kernels, local(): pl.pallas_call(kernel, out_shape=(jax.ShapeDtypeStruct((rows, half), BF16...  137 us
    pallas_call x1, Pallas kernels, local(): pl.pallas_call(tail, out_shape=(jax.ShapeDtypeStruct((rows, half), BF16),...  7.59 us

commit v1 on v0

--- a/solution.py
+++ b/solution.py
@@ -43,6 +43,13 @@
     return shifted(me, tuple(4 - o for o in place(k)))
 
 
+def named_in_order(me, q, n):
+    k = lax.broadcasted_iota(jnp.int32, (NEP, n), 0)
+    dist = ((k >> 4) & 3, (k >> 2) & 3, k & 3)
+    x, y, z = ((c + dist[AXES[q].index(axis)]) & 3 for axis, c in enumerate(place(me)))
+    return z * 16 + y * 4 + x
+
+
 def nn(a, b):
     return lax.dot_general(a, b, (((1,), (0,)), ((), ())), preferred_element_type=F32)
 
@@ -66,7 +73,7 @@
 
 
 def kernel(
-    ids, gates, order, tok_h, cot_h, wg_h, wu_h, wd_h, sg_h, su_h, sd_h,
+    ids, gates, tok_h, cot_h, wg_h, wu_h, wd_h, sg_h, su_h, sd_h,
     o_tok, o_gate, o_rank, o_gg, o_gu, o_gd, o_nrm, o_dn, o_rs, o_sn, o_sdn,
     meta, meta_in, pick, slot_gate, tok, cot, wg, wu, wd, sg, su, sd,
     raw, b0, b1, b2, c0, c1, c2, w0, w1, w2, v0, v1, v2,
@@ -185,10 +192,11 @@
     later = lax.broadcasted_iota(jnp.int32, (n_tok, n_tok), 1)
     before = jnp.where(later > earlier, 1.0, 0.0).astype(BF16)
     for q in range(3):
+        order = named_in_order(me, q, n_tok)
         named = jnp.zeros((NEP, n_tok), F32)
         gate_t = jnp.zeros((NEP, n_tok), F32)
         for j in range(4):
-            hit = ids[j:j + 1] == order[q]
+            hit = ids[j:j + 1] == order
             named = jnp.where(hit, 1.0, named)
             gate_t = jnp.where(hit, gates[j:j + 1], gate_t)
         rank_t = jnp.where(named > 0.0, nn(named.astype(BF16), before), -1.0)
@@ -668,7 +676,7 @@
 
 
 def tail(
-    ids, gates, order, rank, gate_sum, tok_in, nrm, dn, rs, sn, sdn, gg, gu, gd,
+    ids, gates, rank, gate_sum, tok_in, nrm, dn, rs, sn, sdn, gg, gu, gd,
     o_tok, o_gate, o_gg, o_gu, o_gd, o_sg, o_su, o_sd, o_gn, o_un, o_dn, o_sgn, o_sun, o_sdn,
     bg, bu, bd, i_s, o_s,
 ):
@@ -686,16 +694,17 @@
     for cp in ins:
         cp.start()
     o_tok[...] = tok_in[...]
+    order = named_in_order(lax.axis_index("ep"), 0, rank.shape[1])
     value = jnp.zeros(rank.shape, F32)
     for r in range(CAP):
         value = jnp.where(rank[...] == float(r), gate_sum[:, r:r + 1], value)
     for j in range(4):
-        hit = ids[j:j + 1] == order[0]
+        hit = ids[j:j + 1] == order
         total = jnp.sum(jnp.where(hit, value, 0.0), axis=0, keepdims=True)
         o_gate[j:j + 1] = total / gates[j:j + 1]
     o_sg[...] = rs[0]
     o_su[...] = rs[1]
-    o_sd[...] = rs[2].T
+    o_sd[...] = rs[2]
     o_gn[...] = nrm[0:1]
     o_un[...] = nrm[8:9]
     o_dn[...] = dn[0:1]
@@ -710,13 +719,7 @@
 
 
 def local(tokens, expert_ids, gates, cotangent, w_gate, w_up, w_down, sh_gate, sh_up, sh_down):
-    me = lax.axis_index("ep")
     rows, width = tokens.shape
-    k = lax.broadcasted_iota(jnp.int32, (NEP, 1), 0)
-    dist = place(k)[::-1]
-    order = jnp.stack(
-        [shifted(me, tuple(dist[AXES[q].index(axis)] for axis in range(3))) for q in range(3)]
-    )
     ids_t, gates_t = expert_ids.T, gates.T
 
     vm = pl.BlockSpec(memory_space=pltpu.VMEM)
@@ -738,7 +741,7 @@
             jax.ShapeDtypeStruct((2, 32, 128), F32),
             jax.ShapeDtypeStruct((1, 256), F32),
         ),
-        in_specs=[vm] * 3 + [hbm] * 8,
+        in_specs=[vm] * 2 + [hbm] * 8,
         out_specs=(vm, vm, vm, hbm, hbm, hbm, vm, vm, vm, vm, vm),
         scratch_shapes=[
             pltpu.VMEM((3, 4, 2, 16, rows), F32),
@@ -804,7 +807,7 @@
         compiler_params=pltpu.CompilerParams(
             collective_id=0, has_side_effects=True, vmem_limit_bytes=67043328
         ),
-    )(ids_t, gates_t, order, tokens, cotangent, w_gate[0], w_up[0], w_down[0], sh_gate, sh_up, sh_down)
+    )(ids_t, gates_t, tokens, cotangent, w_gate[0], w_up[0], w_down[0], sh_gate, sh_up, sh_down)
     tok_grad, gate_sum, rank, gg, gu, gd, nrm, dn, rs, sn, sdn = out
     res = pl.pallas_call(
         tail,
@@ -816,7 +819,7 @@
             jax.ShapeDtypeStruct((1, 256, width), F32),
             jax.ShapeDtypeStruct((32, 256), F32),
             jax.ShapeDtypeStruct((32, 256), F32),
-            jax.ShapeDtypeStruct((256, 32), F32),
+            jax.ShapeDtypeStruct((32, 256), F32),
             jax.ShapeDtypeStruct((1, width), F32),
             jax.ShapeDtypeStruct((1, width), F32),
             jax.ShapeDtypeStruct((1, 256), F32),
@@ -824,7 +827,7 @@
             jax.ShapeDtypeStruct((1, 32), F32),
             jax.ShapeDtypeStruct((1, 256), F32),
         ),
-        in_specs=[vm] * 11 + [hbm] * 3,
+        in_specs=[vm] * 10 + [hbm] * 3,
         out_specs=(vm, vm, hbm, hbm, hbm) + (vm,) * 9,
         scratch_shapes=[
             pltpu.VMEM((width, 256), F32),
@@ -832,8 +835,8 @@
             pltpu.VMEM((256, width), F32),
             dma((6,)), dma((6,)),
         ],
-    )(ids_t, gates_t, order, rank, gate_sum, tok_grad, nrm, dn, rs, sn, sdn, gg, gu, gd)
-    return (res[0], res[1].T) + res[2:11] + (res[11][0], res[12][0], res[13][0])
+    )(ids_t, gates_t, rank, gate_sum, tok_grad, nrm, dn, rs, sn, sdn, gg, gu, gd)
+    return (res[0], res[1].T) + res[2:7] + (res[7].T,) + res[8:11] + (res[11][0], res[12][0], res[13][0])
 
 
 def solution(mesh):

time: 148 us -> 146 us (0.986)
  local copies, waits for them, and re-layouts: 2.36 us -> 0 us
    unnamed x1 -> x0, local copies, waits for them, and re-layouts: 1.59 us -> none
where the time goes in v1:
time: 146 us; the launch traced here: 145 us
  Pallas kernels  144 us (99%)
    pallas_call x1, Pallas kernels, local(): pl.pallas_call(kernel, out_shape=(jax.ShapeDtypeStruct((rows, half), BF16...  136 us
    pallas_call x1, Pallas kernels, local(): pl.pallas_call(tail, out_shape=(jax.ShapeDtypeStruct((rows, half), BF16),...  7.59 us

profile of v1, /device:TPU:0, one launch (start us, length us, event | category | flops | bytes accessed | tf_op | source)
XLA Modules:
  0.0 144.8 jit_solution(8351369573016986464)
XLA Ops:
  0.6 136.3 %shard_map.209 = (bf16[256,1024]{1,0:T(8,128)(2,1)}, f32[64,128]{1,0:T(8,128)}, f32[64,256]{1,0:T(8,128)}, f32[2048,256]{1,0:T(8,128)}, f32[2048,256]{1,0:T(8,12...) custom-call(s32[4,256]{1,0:T(4,128)} %bitcast.13, ...), custom_call_target="tpu_custom_call" | custom-call | tf_op jit(solution)/shard_map/pallas_call | solution.py:729
  137.0 7.6 %shard_map.210 = (bf16[256,1024]{1,0:T(8,128)(2,1)}, f32[4,256]{1,0:T(4,128)}, f32[1,2048,256]{2,1,0:T(8,128)}, f32[1,2048,256]{2,1,0:T(8,128)}, f32[1,256,2048]...) custom-call(s32[4,256]{1,0:T(4,128)} %bitcast.14, ...), custom_call_target="tpu_custom_call" | custom-call | tf_op jit(solution)/shard_map/pallas_call | solution.py:812
